TPU v7x, 256 devices: a 4x2x16 block of a 4x16x16 slice. The times are simulated.
256 devices in a mesh: grp: 2 (over y), sp: 16 (over z), tp: 4 (over x), dp: 2 (over core).
Axes of the slice: x: 4, y: 2, z: 16, core: 2. Of those that a mesh axis runs over, the one named last changes fastest.
The devices are a block of a 4x16x16 slice.
Arguments:
- latent: bfloat16 [4, 10240, 2048], P(('grp', 'dp'), ('sp', 'tp')), parts along dimension 0, may hold values from -6 to 6
- cond: bfloat16 [4, 2048], P(('grp', 'dp'), 'sp'), parts along dimension 0, may hold values from -6 to 6
- cond_ctx: bfloat16 [2048], P('sp'), may hold values from -6 to 6
- context: bfloat16 [4, 512, 2048], P(('grp', 'dp'), 'sp'), parts along dimension 0, may hold values from -6 to 6
- w_mod: bfloat16 [3, 2048, 2048], P(None, 'sp', 'tp'), may hold values from -0.125 to 0.125
- norm_gain: float32 [2048], replicated, may hold values from 0.1 to 1.9
- w_query: bfloat16 [2048, 8, 128], P(None, 'tp'), may hold values from -5.347495 to 5.347495
- w_key: bfloat16 [2048, 8, 128], P(None, 'tp'), may hold values from -0.13258252 to 0.13258252
- w_value: bfloat16 [2048, 8, 128], P(None, 'tp'), may hold values from -0.125 to 0.125
- lam: float32 [8], P('tp'), may hold values from 0.3 to 0.8
- head_gain: float32 [128], replicated, may hold values from 0.1 to 1.9
- w_out: bfloat16 [8, 128, 2048], P('tp'), may hold values from -0.1875 to 0.1875
Outputs:
- updated: bfloat16 [4, 10240, 2048], P(('grp', 'dp'), ('sp', 'tp')), parts along dimension 0
There are 2 independent parts, one for each index of `grp`. A program takes and returns all parts, laid end to end along the dimension named above; an argument that names none is the same for every part. Nothing has to cross between parts.
All inputs are finite; a program needn't handle non-finite values.
Results may differ from a plain program's by a relative error of at most 0.008.
Values may be sent and summed in bfloat16 or wider, within the bound.
A program may use at most 64 MiB of HBM per device.

v0:
```python
import functools
import math

import jax
import jax.numpy as jnp
from jax import lax
from jax.sharding import PartitionSpec as P

TOK_DEV = 640
CTX_DEV = 32


EPSILON = 1e-06
HEAD_SCALE = 0.8
KEY_BLOCK = 512


def over_axes(array, axes):
    return functools.reduce(lax.psum, axes, array)


def joined_along(pieces, dim):
    shape = list(pieces.shape[1:])
    shape[dim] *= pieces.shape[0]
    return jnp.moveaxis(pieces, 0, dim).reshape(shape)


def from_everyone(array, axis):
    count = lax.axis_size(axis)
    return lax.all_to_all(
        jnp.broadcast_to(array[None], (count, *array.shape)), axis, 0, 0, tiled=True
    )


def collect(array, axis, dim):
    return joined_along(from_everyone(array, axis), dim)


def modulated_norm(tokens, norm_gain, shift, scale):
    values_f = tokens.astype(jnp.float32)
    normed = values_f * lax.rsqrt(jnp.mean(values_f * values_f, axis=-1, keepdims=True) + EPSILON)
    return (normed * norm_gain * (1.0 + scale) + shift).astype(jnp.bfloat16)


def project_weight(tokens, weight):
    flat_weight = weight.reshape(weight.shape[0], weight.shape[1] * weight.shape[2])
    product = jnp.dot(tokens, flat_weight, preferred_element_type=jnp.float32).astype(jnp.bfloat16)
    return product.reshape(tokens.shape[0], weight.shape[1], weight.shape[2])


def block_size(length):
    size_now = min(length, KEY_BLOCK)
    while length % size_now != 0:
        size_now = size_now - 1
    return size_now


def fold_block(carried, queries, key_rows, key_lift):
    running_max, totals, weighted = carried
    key_width = queries.shape[2] // 2
    first_map = jnp.einsum(
        "qhd,khd->qhk",
        queries[..., :key_width],
        key_rows[..., :key_width],
        preferred_element_type=jnp.float32,
    )
    second_map = jnp.einsum(
        "qhd,khd->qhk",
        queries[..., key_width:],
        key_rows[..., key_width : 2 * key_width],
        preferred_element_type=jnp.float32,
    )
    scores = jnp.stack([first_map, second_map]) * key_width ** (-0.5) + key_lift
    new_max = jnp.maximum(running_max, jnp.max(scores, axis=-1))
    rescale = jnp.exp(running_max - new_max)
    weights = jnp.exp(scores - new_max[..., None])
    totals = totals * rescale + jnp.sum(weights, axis=-1)
    weighted = weighted * rescale[..., None] + jnp.einsum(
        "mqhk,khd->mqhd",
        weights.astype(jnp.bfloat16),
        key_rows[..., 2 * key_width :],
        preferred_element_type=jnp.float32,
    )
    return (new_max, totals, weighted)


def fold_rows(carried, queries, key_rows, key_lift):
    length = key_rows.shape[0]
    size_now = block_size(length)
    if size_now == length:
        return fold_block(carried, queries, key_rows, key_lift)
    key_blocks = key_rows.reshape((length // size_now, size_now) + key_rows.shape[1:])
    lift_blocks = key_lift.reshape(length // size_now, size_now)

    def step_block(state_now, pieces):
        return (fold_block(state_now, queries, pieces[0], pieces[1]), None)

    carried, unused = lax.scan(step_block, carried, (key_blocks, lift_blocks))
    return carried


def on_device(
    latent,
    cond,
    cond_ctx,
    context,
    w_mod,
    norm_gain,
    w_query,
    w_key,
    w_value,
    lam,
    head_gain,
    w_out,
):
    lift_value = math.log(TOK_DEV / (4 * CTX_DEV))
    tp_index = lax.axis_index("tp")
    columns = w_mod.shape[2]
    cond_rows = jnp.concatenate(
        [cond.astype(jnp.float32), cond_ctx.astype(jnp.float32)[None]], axis=0
    )
    partial_mod = jnp.einsum(
        "sd,jde->sje",
        jax.nn.silu(cond_rows),
        w_mod.astype(jnp.float32),
        precision=lax.Precision.HIGHEST,
    )
    placed = jnp.zeros((2, 3, columns * lax.axis_size("tp")), jnp.float32)
    placed = lax.dynamic_update_slice(placed, partial_mod, (0, 0, tp_index * columns))
    modulation = over_axes(placed, ("sp", "tp"))
    latent_rows = latent[0]
    normed = modulated_norm(latent_rows, norm_gain, modulation[0, 0], modulation[0, 1])
    ctx_normed = modulated_norm(context[0], norm_gain, modulation[1, 0], modulation[1, 1])
    shard_rows = collect(normed, "tp", 0)
    projected = jnp.concatenate(
        [
            project_weight(shard_rows, w_query),
            project_weight(shard_rows, w_key),
            project_weight(shard_rows, w_value),
        ],
        axis=-1,
    )
    query_width = w_query.shape[2]
    queries = projected[..., :query_width]
    own_keys = projected[..., query_width:]
    ctx_keys = jnp.concatenate(
        [project_weight(ctx_normed, w_key), project_weight(ctx_normed, w_value)], axis=-1
    )
    query_rows = queries.shape[0]
    head_count = queries.shape[1]
    value_width = w_value.shape[2]
    initial = (
        jnp.full((2, query_rows, head_count), -1e30, jnp.float32),
        jnp.zeros((2, query_rows, head_count), jnp.float32),
        jnp.zeros((2, query_rows, head_count, value_width), jnp.float32),
    )
    gathered_ctx = collect(ctx_keys, "sp", 0)
    started = fold_rows(
        initial, queries, gathered_ctx, jnp.full((gathered_ctx.shape[0],), lift_value, jnp.float32)
    )
    shard_rows = lax.all_gather(own_keys, "sp", axis=0, tiled=True)
    folded = fold_rows(started, queries, shard_rows, jnp.zeros((shard_rows.shape[0],), jnp.float32))
    running_max, totals, weighted = folded
    map_outs = weighted / totals[..., None]
    differ = map_outs[0] - lam[None, :, None] * map_outs[1]
    normed_heads = differ * lax.rsqrt(jnp.mean(differ * differ, axis=-1, keepdims=True) + EPSILON)
    attended = (normed_heads * head_gain * HEAD_SCALE).astype(jnp.bfloat16)
    own_rows = latent_rows.shape[0]
    whole_out = lax.all_gather(w_out, "tp", axis=0, tiled=True)
    by_rows = lax.all_to_all(attended, "tp", split_axis=0, concat_axis=1, tiled=True)
    mixed = jnp.dot(
        by_rows.reshape(own_rows, -1),
        whole_out.reshape(-1, whole_out.shape[2]),
        preferred_element_type=jnp.float32,
    )
    gate_vector = modulation[0, 2]
    return (latent_rows.astype(jnp.float32) + gate_vector * mixed).astype(jnp.bfloat16)[None]


def solution(mesh):
    return jax.shard_map(
        on_device,
        mesh=mesh,
        in_specs=(
            P(("grp", "dp"), ("sp", "tp"), None),
            P(("grp", "dp"), "sp"),
            P("sp"),
            P(("grp", "dp"), "sp", None),
            P(None, "sp", "tp"),
            P(),
            P(None, "tp", None),
            P(None, "tp", None),
            P(None, "tp", None),
            P("tp"),
            P(),
            P("tp", None, None),
        ),
        out_specs=P(("grp", "dp"), ("sp", "tp"), None),
        check_vma=False,
    )
```

profile of v0, /device:TPU:40, one launch (start us, length us, event | category | flops | bytes accessed | tf_op | source)
XLA Modules:
  0.0 385.9 jit_solution(13297970081521624862)
XLA Ops:
  6.6 1.0 copy-done
  8.5 75.0 %psum.14 = f32[2,3,2048]{2,0,1:T(2,128)S(1)} all-reduce(f32[2,3,2048]{2,0,1:T(2,128)S(1)} %convolution_dynamic-update-slice_fusion), channel_id=1, replica_groups=mesh['grp'=2,'sp'=16,'tp'=4,'dp'=2] {'sp'}, use_global_device_ids=true, to_apply=%region_0.1 | all-reduce | flops 12288 | bytes 98304 | tf_op jit(solution)/shard_map/psum | solution.py:19
  83.5 18.5 %psum.15 = f32[2,3,2048]{2,0,1:T(2,128)S(1)} all-reduce(f32[2,3,2048]{2,0,1:T(2,128)S(1)} %psum.14), channel_id=1, replica_groups=mesh['grp'=2,'sp'=16,'tp'=4,'dp'=2] {'tp'}, use_global_device_ids=true, to_apply=%region_1.2 | all-reduce | flops 12288 | bytes 98304 | tf_op jit(solution)/shard_map/psum | solution.py:19
  102.1 1.3 fusion.31
  103.4 1.4 fusion.46
  105.1 22.0 %all_to_all.25 = bf16[4,160,2048]{2,1,0:T(8,128)(2,1)S(1)} all-to-all(bf16[4,160,2048]{2,1,0:T(8,128)(2,1)S(1)} %broadcast_in_dim.21), channel_id=1, replica_groups=mesh['grp'=2,'sp'=16,'tp'=4,'dp'=2] {'tp'}, dimensions={0} | all-to-all | bytes 5242880 | tf_op jit(solution)/shard_map/all_to_all | solution.py:30
  127.1 1.8 convolution_convert_fusion.1
  128.9 1.2 copy.75
  130.1 3.0 convolution_convert_fusion
  133.1 1.9 copy.76
  135.0 1.9 pad_maximum_fusion
  137.1 1.6 convolution_convert_fusion.4
  138.6 1.6 convolution_convert_fusion.3
  141.2 4.6 %all-to-all-start = ((bf16[16,32,2,256]{3,1,2,0:T(8,128)(2,1)}), bf16[16,32,2,256]{3,1,2,0:T(8,128)(2,1)}, u32[]{:S(2)}, u32[]{:S(2)}) async-start(bf16[16,32,2,256]{3,1,2,0:T(8,128)(2,1)} %broadcast_in_dim.19), calls=%async_computation | async-start | bytes 1048576 | tf_op jit(solution)/shard_map/all_to_all | solution.py:30
  146.6 2.2 convolution_convert_fusion.2
  148.8 20.7 %all-to-all-done = bf16[16,32,2,256]{3,1,2,0:T(8,128)(2,1)} async-done(((bf16[16,32,2,256]{3,1,2,0:T(8,128)(2,1)}), bf16[16,32,2,256]{3,1,2,0:T(8,128)(2,1)}, u32[]{:S(2)}, u32[]{:S(2)}) %all-to-all-start) | async-done | bytes 524320 | tf_op jit(solution)/shard_map/all_to_all | solution.py:30
  169.5 1.1 copy.69
  172.2 1.2 fusion.16
  174.0 90.0 %all-gather.3.cloned.1.call-done = bf16[10240,2,256]{2,0,1:T(8,128)(2,1)} async-done(((bf16[640,2,256]{2,0,1:T(8,128)(2,1)}), bf16[10240,2,256]{2,0,1:T(8,128)(2,1)}) %all-gather.3.cloned.1.call-update) | async-done | bytes 10485776 | tf_op jit(solution)/shard_map/all_gather | solution.py:161
  264.1 93.8 %while.14 = (s32[]{:T(128)}, f32[2,640,2]{1,2,0:T(2,128)S(1)}, f32[2,640,2]{1,2,0:T(2,128)S(1)}, f32[2,640,2,128]{1,3,0,2:T(8,128)S(1)}, bf16[20,512,2,256]{3,1,...) while((s32[]{:T(128)}, f32[2,640,2]{1,2,0:T(2,128)S(1)}, f32[2,640,2]{1,2,0:T(2,128)S(1)}, ...), condition=%wide.region_9.10_spmd, body=%wide.region_6.9_spmd.sunk | while | flops 514462720 | bytes 26716240 | solution.py:98
  264.1 1.1 constant_dynamic-slice_fusion.2
  266.9 1.0 fusion.94
  268.8 1.1 constant_dynamic-slice_fusion.2
  271.6 1.0 fusion.94
  273.4 1.1 constant_dynamic-slice_fusion.2
  276.3 1.0 fusion.94
  278.1 1.1 constant_dynamic-slice_fusion.2
  281.0 1.0 fusion.94
  282.9 1.1 constant_dynamic-slice_fusion.2
  285.7 1.0 fusion.94
  287.5 1.1 constant_dynamic-slice_fusion.2
  290.3 1.0 fusion.94
  292.2 1.1 constant_dynamic-slice_fusion.2
  295.0 1.0 fusion.94
  296.9 1.1 constant_dynamic-slice_fusion.2
  299.7 1.0 fusion.94
  301.6 1.1 constant_dynamic-slice_fusion.2
  304.4 1.0 fusion.94
  306.3 1.1 constant_dynamic-slice_fusion.2
  309.1 1.0 fusion.94
  311.0 1.1 constant_dynamic-slice_fusion.2
  313.8 1.0 fusion.94
  315.6 1.1 constant_dynamic-slice_fusion.2
  318.5 1.0 fusion.94
  320.3 1.1 constant_dynamic-slice_fusion.2
  323.1 1.0 fusion.94
  325.0 1.1 constant_dynamic-slice_fusion.2
  327.8 1.0 fusion.94
  329.7 1.1 constant_dynamic-slice_fusion.2
  332.5 1.0 fusion.94
  334.4 1.1 constant_dynamic-slice_fusion.2
  337.2 1.0 fusion.94
  339.1 1.1 constant_dynamic-slice_fusion.2
  341.9 1.0 fusion.94
  343.8 1.1 constant_dynamic-slice_fusion.2
  346.6 1.0 fusion.94
  348.5 1.1 constant_dynamic-slice_fusion.2
  351.3 1.0 fusion.94
  353.2 1.1 constant_dynamic-slice_fusion.2
  356.0 1.0 fusion.94
  357.9 1.4 copy.79
  359.5 1.7 broadcast_divide_fusion
  363.2 11.3 %all_to_all.26 = bf16[640,2,128]{2,1,0:T(2,128)(2,1)S(1)} all-to-all(bf16[640,2,128]{2,1,0:T(2,128)(2,1)S(1)} %multiply_convert_fusion), channel_id=1, replica_groups=mesh['grp'=2,'sp'=16,'tp'=4,'dp'=2] {'tp'}, dimensions={0} | all-to-all | bytes 655360 | tf_op jit(solution)/shard_map/all_to_all | solution.py:170
  375.1 3.9 %fusion.22 = bf16[1,160,2048]{2,1,0:T(8,128)(2,1)} fusion(bf16[160,1024]{1,0:T(8,128)(2,1)S(1)} %reshape.188, bf16[1024,2048]{1,0:T(8,128)(2,1)} %bitcast.121, bf16[1,160,2048]{2,1,0:T(8,128)(2,1)S(1)} %copy-done.1, f32[2048]{0:T(1024)S(1)} %bitcast.132), kind=kOutput, calls=%fused_computation.29 | convolution fusion | flops 672399360 | bytes 5840896 | tf_op jit(solution)/shard_map/dot_general | solution.py:171
  (224 shorter events, 58.4 us)
Async XLA Ops:
  6.5 1.0 copy-start
  6.6 257.5 %all-gather.3.cloned.1.call-start = ((), (), s32[]{:S(2)}) async-start(), calls=%async_computation.3 | async-start | bytes 11141120 | tf_op jit(solution)/shard_map/all_gather | solution.py:161
  105.1 22.0 %copy-start.6 = (bf16[2048,2,128]{2,1,0:T(2,128)(2,1)S(1)}, bf16[2048,2,128]{2,1,0:T(2,128)(2,1)}, u32[]{:S(2)}) copy-start(bf16[2048,2,128]{2,1,0:T(2,128)(2,1)} %param.21) | copy-start | bytes 3145732
  130.1 6.8 %copy-start.2 = (bf16[1,32,2048]{2,1,0:T(8,128)(2,1)S(1)}, bf16[1,32,2048]{2,1,0:T(8,128)(2,1)}, u32[]{:S(2)}) copy-start(bf16[1,32,2048]{2,1,0:T(8,128)(2,1)} %param.17) | copy-start | bytes 393220
  130.1 7.0 %copy-start.3 = (f32[2048]{0:T(1024)S(1)}, f32[2048]{0:T(1024)}, u32[]{:S(2)}) copy-start(f32[2048]{0:T(1024)} %param.19) | copy-start | bytes 24580
  141.2 28.4 %all-to-all-start = ((bf16[16,32,2,256]{3,1,2,0:T(8,128)(2,1)}), bf16[16,32,2,256]{3,1,2,0:T(8,128)(2,1)}, u32[]{:S(2)}, u32[]{:S(2)}) async-start(bf16[16,32,2,256]{3,1,2,0:T(8,128)(2,1)} %broadcast_in_dim.19), calls=%async_computation | async-start | bytes 1048576 | tf_op jit(solution)/shard_map/all_to_all | solution.py:30
  145.8 229.3 %all-gather.5.cloned.1.call-start = ((), (), s32[]{:S(2)}) async-start(), calls=%async_computation.4 | async-start | bytes 5242880 | tf_op jit(solution)/shard_map/all_gather | solution.py:169
  359.2 2.0 copy-start.4
  359.5 2.8 copy-start.5
  362.2 12.9 %copy-start.1 = (bf16[1,160,2048]{2,1,0:T(8,128)(2,1)S(1)}, bf16[1,160,2048]{2,1,0:T(8,128)(2,1)}, u32[]{:S(2)}) copy-start(bf16[1,160,2048]{2,1,0:T(8,128)(2,1)} %param.14) | copy-start | bytes 1966084
Sparse Core Ops, SparseCore 0:
  137.0 127.0 all-gather.2
  265.9 52.3 all-gather.4
where the time goes:
time: 388 us; the launch traced here: 386 us
  blocking collectives  127 us (33%)
  waiting for transfers between devices  111 us (29%)
  matrix products  54.2 us (14%)
  other arithmetic  38.8 us (10%)
  local copies, waits for them, and re-layouts  34.8 us (9%)
  between operations  13.7 us (4%)
  starting transfers between devices  4.87 us (1%)
    psum x2, blocking collectives, over_axes(): return functools.reduce(lax.psum, axes, array)  93.5 us
    all_gather x1, waiting for transfers between devices, on_device(): shard_rows = lax.all_gather(own_keys, 'sp', axis=0, tiled=True)  90 us
    dynamic_slice x40, local copies, waits for them, and re-layouts, fold_rows(): carried, unused = lax.scan(step_block, carried, (key_blocks, lift_blocks))  26 us
    all_to_all x1, blocking collectives, from_everyone(): lax.all_to_all(jnp.broadcast_to(array[None], (count, *array.shape)), axis...  22 us
    convert_element_type x21, other arithmetic, fold_block(): weights.astype(jnp.bfloat16)  21.7 us
    all_to_all x1, waiting for transfers between devices, from_everyone(): lax.all_to_all(jnp.broadcast_to(array[None], (count, *array.shape)), axis...  20.7 us
    dot_general x21, matrix products, fold_block(): jnp.einsum('mqhk,khd->mqhd', weights.astype(jnp.bfloat16), key_rows[...,...  16.1 us
    dot_general x21, matrix products, fold_block(): jnp.einsum('qhd,khd->qhk', queries[..., key_width:], key_rows[..., key_wi...  11.6 us
  transfers between devices with their start and end apart: 3, of which 2 were waited for; matrix products, arithmetic and copies ran while one was open for 28% of the time, Pallas kernels for 0%

commit v1 on v0

v1 whole, which is shorter than its diff:
```python
import functools
import math

import jax
import jax.numpy as jnp
from jax import lax
from jax.experimental import pallas as pl
from jax.experimental.pallas import tpu as pltpu
from jax.sharding import PartitionSpec as P

TOK_DEV = 640
CTX_DEV = 32

EPSILON = 1e-06
HEAD_SCALE = 0.8
MESH = pl.DeviceIdType.MESH
QTILE = 256


def remote(src, dst, send, recv, device):
    return pltpu.make_async_remote_copy(
        src_ref=src,
        dst_ref=dst,
        send_sem=send,
        recv_sem=recv,
        device_id=device,
        device_id_type=MESH,
    )


def greet(peers):
    barrier = pltpu.get_barrier_semaphore()
    for peer in peers:
        pl.semaphore_signal(barrier, inc=1, device_id=peer, device_id_type=MESH)
    pl.semaphore_wait(barrier, len(peers))


def exchange_kernel(
    n_sp, n_tp, part, latent, mod, rows, far, near, total, far_s, far_r, near_s, near_r, tp_s, tp_r, lat_s, lat_r, own_s
):
    z = lax.axis_index("sp")
    x = lax.axis_index("tp")
    quarter = n_sp // 4

    def sp_at(offset):
        return {"sp": lax.rem(z + offset + n_sp, n_sp)}

    def tp_at(offset):
        return {"tp": lax.rem(x + offset, n_tp)}

    far_peers = [sp_at(quarter * k) for k in (1, 2, 3)]
    near_peers = [sp_at(1), sp_at(-1), sp_at(2)]
    tp_peers = [tp_at(k) for k in (1, 2, 3)]
    greet(far_peers + near_peers + [sp_at(-2)] + tp_peers)
    right, left = tp_at(1), tp_at(n_tp - 1)
    half = latent.shape[0] // 2
    first, second = pl.ds(0, half), pl.ds(half, half)

    own = pltpu.make_async_copy(latent, rows.at[0], own_s)
    far_copies = [
        remote(part, far.at[k], far_s.at[k], far_r.at[k], far_peers[k]) for k in range(3)
    ]
    for copy in far_copies:
        copy.start()
    to_right = [
        remote(latent.at[part_rows], rows.at[1, part_rows], lat_s.at[k], lat_r.at[k], right)
        for k, part_rows in enumerate((first, second))
    ]
    to_left = [
        remote(latent.at[part_rows], rows.at[2, part_rows], lat_s.at[2 + k], lat_r.at[2 + k], left)
        for k, part_rows in enumerate((second, first))
    ]
    to_right[0].start()
    to_left[0].start()
    to_right[1].start()
    to_left[1].start()
    own.start()
    for copy in far_copies:
        copy.wait_recv()
    total[...] = part[...] + far[0] + far[1] + far[2]
    near_copies = [
        remote(total, near.at[k], near_s.at[k], near_r.at[k], near_peers[k]) for k in range(3)
    ]
    for copy in near_copies:
        copy.start()
    to_right[0].wait_recv()
    onward_right = remote(
        rows.at[1, first], rows.at[3, first], lat_s.at[4], lat_r.at[4], right
    )
    onward_right.start()
    to_left[0].wait_recv()
    onward_left = remote(
        rows.at[2, second], rows.at[3, second], lat_s.at[5], lat_r.at[5], left
    )
    onward_left.start()
    for copy in near_copies:
        copy.wait_recv()
    columns = part.shape[1]
    mine = pl.ds(pl.multiple_of(x * columns, columns), columns)
    mod[:, mine] = total[...] + near[0] + near[1] + near[2]
    tp_copies = [
        remote(mod.at[:, mine], mod.at[:, mine], tp_s.at[k], tp_r.at[k], tp_peers[k])
        for k in range(3)
    ]
    for copy in tp_copies:
        copy.start()
    for k in range(3):
        source = lax.rem(x + n_tp - 1 - k, n_tp)
        theirs = pl.ds(pl.multiple_of(source * columns, columns), columns)
        remote(mod.at[:, theirs], mod.at[:, theirs], tp_s.at[k], tp_r.at[k], tp_peers[k]).wait_recv()
    to_right[1].wait_recv()
    to_left[1].wait_recv()
    onward_right.wait_recv()
    onward_left.wait_recv()
    own.wait()
    for copy in far_copies + near_copies + tp_copies + to_right + to_left + [onward_right, onward_left]:
        copy.wait_send()


def exchange(n_sp, n_tp, part, latent):
    dma = pltpu.SemaphoreType.DMA
    vmem = pl.BlockSpec(memory_space=pltpu.VMEM)
    return pl.pallas_call(
        functools.partial(exchange_kernel, n_sp, n_tp),
        out_shape=(
            jax.ShapeDtypeStruct((part.shape[0], part.shape[1] * n_tp), jnp.float32),
            jax.ShapeDtypeStruct((n_tp,) + latent.shape, latent.dtype),
        ),
        in_specs=[vmem] * 2,
        out_specs=(vmem, vmem),
        scratch_shapes=[
            pltpu.VMEM((3,) + part.shape, jnp.float32),
            pltpu.VMEM((3,) + part.shape, jnp.float32),
            pltpu.VMEM(part.shape, jnp.float32),
            dma((3,)),
            dma((3,)),
            dma((3,)),
            dma((3,)),
            dma((3,)),
            dma((3,)),
            dma((6,)),
            dma((6,)),
            dma,
        ],
        compiler_params=pltpu.CompilerParams(collective_id=0, has_side_effects=True),
        name="exchange",
    )(part, latent)


def attend_kernel(
    n_sp, n_tp, n_ctx, lift, kv, q_t, lam, head_gain, w_out, latent, gate, out,
    blocks, w_far, q_wide, acc, top, total, v_t, att, got,
    own_s, ring_s, ring_r, w_s, w_r, att_s, att_r,
):
    z = lax.axis_index("sp")
    x = lax.axis_index("tp")
    length = kv.shape[0]
    chunk = length // 2
    heads = lam.shape[0]
    width = head_gain.shape[0]
    n_query = q_t.shape[1]
    tiles = 2 * n_query // QTILE
    last = n_sp - 2

    def sp_to(direction):
        return {"sp": lax.rem(z + 1 - 2 * direction + n_sp, n_sp)}

    def tp_at(offset):
        return {"tp": lax.rem(x + offset, n_tp)}

    tp_peers = [tp_at(k) for k in (1, 2, 3)]
    greet([sp_to(0), sp_to(1)] + tp_peers)
    right, left = tp_peers[0], tp_peers[2]

    own_copies = []
    for c in range(2):
        for d in range(2):
            span = pl.ds(c * chunk, chunk)
            own_copies.append(
                remote(kv.at[span], blocks.at[d, span], own_s.at[d, c], ring_r.at[d, c], sp_to(d))
            )
    for copy in own_copies:
        copy.start()
    w_rows = w_out.shape[0]
    upper, lower = pl.ds(0, w_rows // 2), pl.ds(w_rows // 2, w_rows // 2)
    w_right = remote(w_out, w_far.at[0], w_s.at[0], w_r.at[0], right)
    w_left = remote(w_out, w_far.at[2], w_s.at[1], w_r.at[1], left)
    w_right_on = remote(w_far.at[0, upper], w_far.at[1, upper], w_s.at[2], w_r.at[2], right)
    w_left_on = remote(w_far.at[2, lower], w_far.at[1, lower], w_s.at[3], w_r.at[3], left)
    w_right.start()
    w_left.start()

    q_wide[...] = jnp.zeros_like(q_wide)
    half_width = width // 2
    for h in range(heads):
        for m in range(2):
            span = slice(h * width + m * half_width, h * width + (m + 1) * half_width)
            q_wide[span, m * n_query : (m + 1) * n_query] = q_t[span, :]
    acc[...] = jnp.zeros_like(acc)
    total[...] = jnp.zeros_like(total)
    top[...] = jnp.full_like(top, -1e30)

    def fold(block):
        def head(h, carry):
            base = pl.multiple_of(h * width, width)
            keys = block[:, pl.ds(base, width)]
            v_t[...] = block[:, pl.ds(pl.multiple_of(heads * width + base, width), width)].T
            for j in range(tiles):
                columns = slice(j * QTILE, (j + 1) * QTILE)
                scores = jnp.dot(
                    keys, q_wide[pl.ds(base, width), columns], preferred_element_type=jnp.float32
                )
                scores = jnp.concatenate(
                    [scores[: length - n_ctx], scores[length - n_ctx :] + lift], axis=0
                )
                old = top[h, :, columns]
                new = jnp.maximum(old, jnp.max(scores, axis=0, keepdims=True))
                weights = jnp.exp(scores - new)
                rescale = jnp.exp(old - new)
                top[h, :, columns] = new
                total[h, :, columns] = total[h, :, columns] * rescale + jnp.sum(
                    weights, axis=0, keepdims=True
                )
                acc[h, :, columns] = acc[h, :, columns] * rescale + jnp.dot(
                    v_t[...], weights.astype(jnp.bfloat16), preferred_element_type=jnp.float32
                )
            return carry

        lax.fori_loop(0, heads, head, 0)

    def ring_copy(t, c):
        span = pl.ds(c * chunk, chunk)
        target = jnp.minimum(t + 2, last)
        return remote(
            blocks.at[t, span],
            blocks.at[target, span],
            ring_s.at[t, c],
            ring_r.at[target, c],
            sp_to(lax.rem(t, 2)),
        )

    def arrival(t, c):
        span = pl.ds(c * chunk, chunk)
        return remote(
            blocks.at[t, span], blocks.at[t, span], ring_s.at[t, c], ring_r.at[t, c], sp_to(0)
        )

    def forwards(t, c):
        return jnp.logical_or(t < last - 2, t == last - 2 + c)

    fold(kv)

    def ring_step(t, carry):
        for c in range(2):
            arrival(t, c).wait_recv()

            @pl.when(forwards(t, c))
            def _():
                ring_copy(t, c).start()

        @pl.when(t == 6)
        def _():
            w_right.wait_recv()
            w_right_on.start()
            w_left.wait_recv()
            w_left_on.start()

        fold(blocks.at[t])
        return carry

    lax.fori_loop(0, last + 1, ring_step, 0)

    for h in range(heads):
        first = acc[h, :, :n_query] / total[h, :, :n_query]
        second = acc[h, :, n_query:] / total[h, :, n_query:]
        differ = first - lam[h] * second
        scale = lax.rsqrt(jnp.mean(differ * differ, axis=0, keepdims=True) + EPSILON)
        normed = differ * scale * head_gain[...] * HEAD_SCALE
        att[:, h * width : (h + 1) * width] = normed.T.astype(jnp.bfloat16)

    own_rows = latent.shape[0]
    slot_of = {1: 2, 2: 3, 3: 1}
    sends = []
    for k in (1, 2, 3):
        sends.append(
            remote(
                att.at[pl.ds(slot_of[k] * own_rows, own_rows)],
                got.at[k - 1],
                att_s.at[k - 1],
                att_r.at[k - 1],
                tp_peers[k - 1],
            )
        )
    for copy in sends:
        copy.start()
    w_right_on.wait_recv()
    w_left_on.wait_recv()
    for copy in sends:
        copy.wait_recv()
    n_columns = latent.shape[1]
    step = 512
    for j in range(n_columns // step):
        columns = slice(j * step, (j + 1) * step)
        mixed = jnp.dot(att[:own_rows, :], w_out[:, columns], preferred_element_type=jnp.float32)
        for k in range(3):
            mixed += jnp.dot(got[k], w_far[k, :, columns], preferred_element_type=jnp.float32)
        out[:, columns] = (
            latent[:, columns].astype(jnp.float32) + gate[:, columns] * mixed
        ).astype(out.dtype)

    for copy in own_copies + [w_right, w_left, w_right_on, w_left_on] + sends:
        copy.wait_send()

    def drain(t, carry):
        for c in range(2):

            @pl.when(forwards(t, c))
            def _():
                ring_copy(t, c).wait_send()

        return carry

    lax.fori_loop(0, last + 1, drain, 0)


def attend(n_sp, n_tp, n_ctx, lift, kv, q_t, lam, head_gain, w_out, latent, gate):
    dma = pltpu.SemaphoreType.DMA
    vmem = pl.BlockSpec(memory_space=pltpu.VMEM)
    heads, width, n_query = lam.shape[0], head_gain.shape[0], q_t.shape[1]
    length = kv.shape[0]
    return pl.pallas_call(
        functools.partial(attend_kernel, n_sp, n_tp, n_ctx, lift),
        out_shape=jax.ShapeDtypeStruct(latent.shape, latent.dtype),
        in_specs=[vmem, vmem, pl.BlockSpec(memory_space=pltpu.SMEM)] + [vmem] * 4,
        out_specs=vmem,
        scratch_shapes=[
            pltpu.VMEM((n_sp - 1,) + kv.shape, kv.dtype),
            pltpu.VMEM((3,) + w_out.shape, w_out.dtype),
            pltpu.VMEM((heads * width, 2 * n_query), jnp.bfloat16),
            pltpu.VMEM((heads, width, 2 * n_query), jnp.float32),
            pltpu.VMEM((heads, 1, 2 * n_query), jnp.float32),
            pltpu.VMEM((heads, 1, 2 * n_query), jnp.float32),
            pltpu.VMEM((width, length), jnp.bfloat16),
            pltpu.VMEM((n_query, heads * width), jnp.bfloat16),
            pltpu.VMEM((3, latent.shape[0], heads * width), jnp.bfloat16),
            dma((2, 2)),
            dma((n_sp - 1, 2)),
            dma((n_sp - 1, 2)),
            dma((4,)),
            dma((4,)),
            dma((3,)),
            dma((3,)),
        ],
        compiler_params=pltpu.CompilerParams(
            collective_id=1, has_side_effects=True, vmem_limit_bytes=56 * 1024 * 1024
        ),
        name="attend",
    )(kv, q_t, lam, head_gain, w_out, latent, gate)


def modulated_norm(tokens, norm_gain, shift, scale):
    values_f = tokens.astype(jnp.float32)
    normed = values_f * lax.rsqrt(jnp.mean(values_f * values_f, axis=-1, keepdims=True) + EPSILON)
    return (normed * norm_gain * (1.0 + scale) + shift).astype(jnp.bfloat16)


def flat(weight):
    return weight.reshape(weight.shape[0], weight.shape[1] * weight.shape[2])


def on_device(
    latent, cond, cond_ctx, context, w_mod, norm_gain, w_query, w_key, w_value, lam, head_gain, w_out
):
    n_sp, n_tp = lax.axis_size("sp"), lax.axis_size("tp")
    lift = math.log(TOK_DEV / (4 * CTX_DEV))
    cond_rows = jnp.concatenate(
        [cond.astype(jnp.float32), cond_ctx.astype(jnp.float32)[None]], axis=0
    )
    partial_mod = jnp.einsum(
        "sd,jde->sje",
        jax.nn.silu(cond_rows),
        w_mod.astype(jnp.float32),
        precision=lax.Precision.HIGHEST,
    )
    columns = w_mod.shape[2]
    part = jnp.concatenate(
        [partial_mod.reshape(6, columns), jnp.zeros((2, columns), jnp.float32)], axis=0
    )
    modulation, rows = exchange(n_sp, n_tp, part, latent[0])
    rows = rows.reshape(-1, rows.shape[2])
    normed = modulated_norm(rows, norm_gain, modulation[0], modulation[1])
    ctx_normed = modulated_norm(context[0], norm_gain, modulation[3], modulation[4])
    tokens = jnp.concatenate([normed, ctx_normed], axis=0)
    keys = jnp.dot(tokens, flat(w_key), preferred_element_type=jnp.float32)
    values = jnp.dot(tokens, flat(w_value), preferred_element_type=jnp.float32)
    kv = jnp.concatenate([keys.astype(jnp.bfloat16), values.astype(jnp.bfloat16)], axis=1)
    half = w_query.shape[2] // 2
    q_t = lax.dot_general(
        flat(w_query), normed, (((0,), (1,)), ((), ())), preferred_element_type=jnp.float32
    )
    q_t = q_t.astype(jnp.bfloat16) * jnp.bfloat16(half ** (-0.5))
    updated = attend(
        n_sp,
        n_tp,
        context.shape[1],
        lift,
        kv,
        q_t,
        lam,
        head_gain[:, None],
        w_out.reshape(-1, w_out.shape[2]),
        latent[0],
        modulation[2:3],
    )
    return updated[None]


def solution(mesh):
    return jax.shard_map(
        on_device,
        mesh=mesh,
        in_specs=(
            P(("grp", "dp"), ("sp", "tp"), None),
            P(("grp", "dp"), "sp"),
            P("sp"),
            P(("grp", "dp"), "sp", None),
            P(None, "sp", "tp"),
            P(),
            P(None, "tp", None),
            P(None, "tp", None),
            P(None, "tp", None),
            P("tp"),
            P(),
            P("tp", None, None),
        ),
        out_specs=P(("grp", "dp"), ("sp", "tp"), None),
        check_vma=False,
    )
```

time: 388 us -> 202 us (0.52)
  Pallas kernels: 0 us -> 185 us
  blocking collectives: 127 us -> 0 us
  waiting for transfers between devices: 111 us -> 0 us
  matrix products: 54.2 us -> 4.47 us
  other arithmetic: 38.8 us -> 7.31 us
  local copies, waits for them, and re-layouts: 34.8 us -> 4.97 us
  between operations: 13.7 us -> 0.13 us
  starting transfers between devices: 4.87 us -> 0 us
    pallas_call x0 -> x2, Pallas kernels: none -> 185 us  [the longest x1 134 us: attend(): pl.pallas_call(functools.partial(attend_kernel, n_sp, n_tp, n_ctx, lift),...]
    psum x2 -> x0, blocking collectives: 93.5 us -> none  [over_axes(): return functools.reduce(lax.psum, axes, array)]
    all_gather x2 -> x0, waiting for transfers between devices: 90.1 us -> none  [the longest x1 90 us: on_device(): shard_rows = lax.all_gather(own_keys, 'sp', axis=0, tiled=True)]
    dot_general x69 -> x3, matrix products: 53.3 us -> 3.53 us  [the longest x1 1.75 us: on_device(): lax.dot_general(flat(w_query), normed, (((0,), (1,)), ((), ())), preferre...]
    all_to_all x2 -> x0, blocking collectives: 33.3 us -> none  [the longest x1 22 us: from_everyone(): lax.all_to_all(jnp.broadcast_to(array[None], (count, *array.shape)), axis...]
    dynamic_slice x40 -> x0, local copies, waits for them, and re-layouts: 26 us -> none  [fold_rows(): carried, unused = lax.scan(step_block, carried, (key_blocks, lift_blocks))]
    all_to_all x1 -> x0, waiting for transfers between devices: 20.7 us -> none  [from_everyone(): lax.all_to_all(jnp.broadcast_to(array[None], (count, *array.shape)), axis...]
    convert_element_type x22 -> x3, other arithmetic: 22.6 us -> 2.18 us  [modulated_norm(): return (normed * norm_gain * (1.0 + scale) + shift).astype(jnp.bfloat16)]
  transfers between devices with their start and end apart: 3 -> 0, of which waited for: 2 -> 0; matrix products, arithmetic and copies ran while one was open for 28% -> 0% of each run, Pallas kernels for 0% -> 0%
where the time goes in v1:
time: 202 us
  Pallas kernels  185 us (92%)
  other arithmetic  7.31 us (4%)
  local copies, waits for them, and re-layouts  4.97 us (2%)
  matrix products  4.47 us (2%)
    pallas_call x1, Pallas kernels, attend(): pl.pallas_call(functools.partial(attend_kernel, n_sp, n_tp, n_ctx, lift),...  134 us
    pallas_call x1, Pallas kernels, exchange(): pl.pallas_call(functools.partial(exchange_kernel, n_sp, n_tp), out_shape=...  50.8 us

profile of v1, /device:TPU:40, one launch (start us, length us, event | category | flops | bytes accessed | tf_op | source)
XLA Modules:
  0.0 201.7 jit_solution(15074086687146998457)
XLA Ops:
  0.0 0.0 copy-start
  0.0 0.0 copy-start.3
  0.0 1.0 copy-done
  1.0 0.9 fusion.24
  2.0 0.6 concatenate.17.part
  2.6 50.8 %exchange.1 = (f32[8,2048]{1,0:T(8,128)}, bf16[4,160,2048]{2,1,0:T(8,128)(2,1)}) custom-call(f32[8,512]{1,0:T(8,128)} %concatenate.17.part, bf16[160,2048]{1,0:T(8,128)(2,1)} %bitcast.44), custom_call_target="tpu_custom_call" | custom-call | tf_op jit(solution)/shard_map/exchange/pallas_call | solution.py:123
  53.4 0.0 copy-start.1
  53.4 1.7 fusion.34
  55.2 2.3 %multiply_reduce_fusion = f32[4,160]{1,0:T(4,128)S(1)} fusion(bf16[4,160,2048]{2,1,0:T(8,128)(2,1)} %get-tuple-element.7), kind=kLoop, calls=%fused_computation.6 | loop fusion | flops 3931520 | bytes 2624000 | tf_op jit(solution)/shard_map/reduce_sum | solution.py:363
  57.5 0.1 rsqrt.21
  57.6 0.0 copy-done.3
  57.6 0.0 copy-done.1
  57.6 0.0 copy-start.2
  57.6 0.0 copy-start.5
  57.7 1.0 fusion.3
  58.7 0.0 copy-done.2
  58.7 0.1 fusion.16
  58.9 0.1 fusion.20
  59.0 0.0 copy-done.5
  59.0 0.0 copy-start.6
  59.0 0.9 fusion.6
  59.9 0.3 copy-done.6
  60.2 0.9 fusion.7
  61.1 0.9 pad_maximum_fusion.7.kv
  62.0 0.0 copy-start.7
  62.0 1.0 add_convert_fusion
  63.1 0.0 copy-start.4
  63.1 0.2 copy-done.7
  63.3 1.7 fusion.9.q_t
  65.0 0.0 copy-done.4
  65.0 0.7 copy.18.head_gain
  65.7 134.0 %attend.1 = bf16[160,2048]{1,0:T(8,128)(2,1)} custom-call(bf16[672,512]{1,0:T(8,128)(2,1)} %pad_maximum_fusion.7.kv, bf16[256,640]{1,0:T(8,128)(2,1)} %fusion.9.q_t, f32[2]{0:T(128)} %lam.1, f32[128,1]{1,0:T(8,128)} %copy.18.head_gain, bf16[256,2048]{1,0:T(8,128)(2,1)} %bitcast.47, bf16[160,2048]{1,0:T(8,128)(2,1)} %bitcast.45, f32[1,2048]{1,0:T(1,128)} %get-tuple-element.9.gate), custom_call_target="tpu_custom_call" | custom-call | tf_op jit(solution)/shard_map/attend/pallas_call | solution.py:331
  199.7 2.0 copy.36
  (4 shorter events, 0.0 us)
Async XLA Ops:
  0.0 1.0 copy-start
  0.0 57.6 %copy-start.3 = (f32[2048]{0:T(1024)S(1)}, f32[2048]{0:T(1024)}, u32[]{:S(2)}) copy-start(f32[2048]{0:T(1024)} %param.17) | copy-start | bytes 24580
  53.4 4.2 %copy-start.1 = (bf16[4,160,2048]{2,1,0:T(8,128)(2,1)S(1)}, bf16[4,160,2048]{2,1,0:T(8,128)(2,1)}, u32[]{:S(2)}) copy-start(bf16[4,160,2048]{2,1,0:T(8,128)(2,1)} %get-tuple-element.7) | copy-start | bytes 7864324
  57.6 1.1 copy-start.2
  57.6 1.3 copy-start.5
  59.0 1.2 copy-start.6
  62.0 1.2 copy-start.7
  63.1 1.9 copy-start.4

commit v2 on v1

v2 whole, which is shorter than its diff:
```python
import functools
import math

import jax
import jax.numpy as jnp
from jax import lax
from jax.experimental import pallas as pl
from jax.experimental.pallas import tpu as pltpu
from jax.sharding import PartitionSpec as P

TOK_DEV = 640
CTX_DEV = 32

EPSILON = 1e-06
HEAD_SCALE = 0.8
MESH = pl.DeviceIdType.MESH
QTILE = 256


def remote(src, dst, send, recv, device):
    return pltpu.make_async_remote_copy(
        src_ref=src,
        dst_ref=dst,
        send_sem=send,
        recv_sem=recv,
        device_id=device,
        device_id_type=MESH,
    )


def greet(peers):
    barrier = pltpu.get_barrier_semaphore()
    for peer in peers:
        pl.semaphore_signal(barrier, inc=1, device_id=peer, device_id_type=MESH)
    pl.semaphore_wait(barrier, len(peers))


def fused_kernel(
    n_sp, n_tp, lift,
    part, latent, context, norm_gain, w_query, w_key, w_value, lam, head_gain, w_out, out,
    far, near, sums, mod, rows, w_raw, w_kv, w_q, w_own, w_far, tokens, queries,
    blocks, q_wide, acc, top, total, v_t, att, got,
    far_s, far_r, near_s, near_r, tp_s, tp_r, lat_s, lat_r, load_s, ring_s, ring_r, w_s, w_r, att_s, att_r,
):
    z = lax.axis_index("sp")
    x = lax.axis_index("tp")
    own_rows, n_ctx = latent.shape[0], context.shape[0]
    heads = lam.shape[0]
    width = head_gain.shape[0]
    n_query = n_tp * own_rows
    length = n_query + n_ctx
    tiles = 2 * n_query // QTILE
    steps = n_sp // 2
    starts = [0] + [n_ctx + k * own_rows for k in range(1, n_tp)]
    sizes = [n_ctx + own_rows] + [own_rows] * (n_tp - 1)

    def sp_at(offset):
        return {"sp": lax.rem(z + offset + n_sp, n_sp)}

    def tp_at(offset):
        return {"tp": lax.rem(x + offset, n_tp)}

    quarter = n_sp // 4
    far_peers = [sp_at(quarter * k) for k in (1, 2, 3)]
    near_peers = [sp_at(1), sp_at(-1), sp_at(2)]
    tp_peers = [tp_at(k) for k in (1, 2, 3)]
    right, left = tp_peers[0], tp_peers[2]
    ring_peers = [sp_at(1), sp_at(-1)]

    raw = [w_key, w_value, w_query]
    raw_loads = [pltpu.make_async_copy(raw[k], w_raw.at[k], load_s.at[k]) for k in range(3)]
    out_load = pltpu.make_async_copy(w_out, w_own, load_s.at[3])
    for copy in raw_loads + [out_load]:
        copy.start()
    greet(far_peers + near_peers + [sp_at(-2)] + tp_peers)

    far_copies = [
        remote(part, far.at[k], far_s.at[k], far_r.at[k], far_peers[k]) for k in range(3)
    ]
    for copy in far_copies:
        copy.start()

    half = own_rows // 2
    piece = 48

    def send_rows(k, slot, first, count, peer):
        span = pl.ds(first, count)
        return remote(latent.at[span], rows.at[slot, span], lat_s.at[k], lat_r.at[k], peer)

    to_right = [
        send_rows(0, 0, 0, half, right),
        send_rows(1, 0, half, piece, right),
        send_rows(2, 0, half + piece, half - piece, right),
    ]
    to_left = [
        send_rows(3, 1, half, half, left),
        send_rows(4, 1, 0, piece, left),
        send_rows(5, 1, piece, half - piece, left),
    ]
    first, second = pl.ds(0, half), pl.ds(half, half)
    onward_right = remote(rows.at[0, first], rows.at[2, first], lat_s.at[6], lat_r.at[6], right)
    onward_left = remote(rows.at[1, second], rows.at[2, second], lat_s.at[7], lat_r.at[7], left)
    for k in range(2):
        to_right[k].start()
        to_left[k].start()

    q_wide[...] = jnp.zeros_like(q_wide)
    acc[...] = jnp.zeros_like(acc)
    total[...] = jnp.zeros_like(total)
    top[...] = jnp.full_like(top, -1e30)
    for k in range(2):
        raw_loads[k].wait()
        for h in range(heads):
            column = (k * heads + h) * width
            w_kv[:, column : column + width] = w_raw[k, :, h, :]

    for copy in far_copies:
        copy.wait_recv()
    sums[...] = part[...] + far[0] + far[1] + far[2]
    near_copies = [
        remote(sums, near.at[k], near_s.at[k], near_r.at[k], near_peers[k]) for k in range(3)
    ]
    for copy in near_copies:
        copy.start()
    raw_loads[2].wait()
    for h in range(heads):
        w_q[:, h * width : (h + 1) * width] = w_raw[2, :, h, :]
    for copy in near_copies:
        copy.wait_recv()
    columns = part.shape[1]

    def mod_of(owner):
        span = pl.ds(pl.multiple_of(owner * columns, columns), columns)
        return mod.at[:, span]

    mine = pl.ds(pl.multiple_of(x * columns, columns), columns)
    mod[:, mine] = sums[...] + near[0] + near[1] + near[2]
    tp_copies = [
        remote(mod_of(x), mod_of(x), tp_s.at[k], tp_r.at[k], tp_peers[k]) for k in range(3)
    ]
    for copy in tp_copies:
        copy.start()
    to_right[2].start()
    to_left[2].start()
    to_right[0].wait_recv()
    onward_right.start()
    to_left[0].wait_recv()
    onward_left.start()
    for k in range(3):
        theirs = mod_of(lax.rem(x + n_tp - 1 - k, n_tp))
        remote(theirs, theirs, tp_s.at[k], tp_r.at[k], tp_peers[k]).wait_recv()

    def norm(source, target, count, kind):
        gain = norm_gain[...] * (1.0 + mod[kind + 1 : kind + 2, :])
        shift = mod[kind : kind + 1, :]
        group = 16

        def some(i, carry):
            span = pl.ds(pl.multiple_of(i * group, group), group)
            values = source[span, :].astype(jnp.float32)
            scale = lax.rsqrt(jnp.mean(values * values, axis=-1, keepdims=True) + EPSILON)
            spot = pl.ds(pl.multiple_of(target + i * group, group), group)
            tokens[spot, :] = (values * scale * gain + shift).astype(jnp.bfloat16)
            return carry

        lax.fori_loop(0, count // group, some, 0, unroll=2)

    def ring_copy(slot, target, d, c):
        span = pl.ds(starts[c], sizes[c])
        return remote(
            blocks.at[slot, span],
            blocks.at[target, span],
            ring_s.at[slot, d, c],
            ring_r.at[target, c],
            ring_peers[d],
        )

    def project(c):
        span = slice(starts[c], starts[c] + sizes[c])
        blocks[0, span, :] = jnp.dot(
            tokens[: sizes[c], :], w_kv[...], preferred_element_type=jnp.float32
        ).astype(jnp.bfloat16)
        queries[c * own_rows : (c + 1) * own_rows, :] = jnp.dot(
            tokens[:own_rows, :], w_q[...], preferred_element_type=jnp.float32
        ).astype(jnp.bfloat16)
        for d in range(2):
            ring_copy(0, 1 + d, d, c).start()

    norm(latent, 0, own_rows, 0)
    norm(context, own_rows, n_ctx, 3)
    project(0)
    for k in (1, 2):
        to_right[k].wait_recv()
    norm(rows.at[0], 0, own_rows, 0)
    project(1)
    for k in (1, 2):
        to_left[k].wait_recv()
    norm(rows.at[1], 0, own_rows, 0)
    project(2)
    onward_right.wait_recv()
    onward_left.wait_recv()
    norm(rows.at[2], 0, own_rows, 0)
    project(3)

    w_rows = w_own.shape[0]
    upper, lower = pl.ds(0, w_rows // 2), pl.ds(w_rows // 2, w_rows // 2)
    w_right = remote(w_own, w_far.at[0], w_s.at[0], w_r.at[0], right)
    w_left = remote(w_own, w_far.at[2], w_s.at[1], w_r.at[1], left)
    w_right_on = remote(w_far.at[0, upper], w_far.at[1, upper], w_s.at[2], w_r.at[2], right)
    w_left_on = remote(w_far.at[2, lower], w_far.at[1, lower], w_s.at[3], w_r.at[3], left)
    out_load.wait()
    w_right.start()
    w_left.start()

    half_width = width // 2
    for h in range(heads):
        for m in range(2):
            span = slice(h * width + m * half_width, h * width + (m + 1) * half_width)
            q_wide[span, m * n_query : (m + 1) * n_query] = queries[:, span].T * jnp.bfloat16(
                half_width ** (-0.5)
            )

    def fold(block):
        def head(h, carry):
            base = pl.multiple_of(h * width, width)
            keys = block[:, pl.ds(base, width)]
            v_t[...] = block[:, pl.ds(pl.multiple_of(heads * width + base, width), width)].T
            for j in range(tiles):
                columns = slice(j * QTILE, (j + 1) * QTILE)
                scores = jnp.dot(
                    keys, q_wide[pl.ds(base, width), columns], preferred_element_type=jnp.float32
                )
                scores = jnp.concatenate(
                    [
                        scores[:own_rows],
                        scores[own_rows : own_rows + n_ctx] + lift,
                        scores[own_rows + n_ctx :],
                    ],
                    axis=0,
                )
                old = top[h, :, columns]
                new = jnp.maximum(old, jnp.max(scores, axis=0, keepdims=True))
                weights = jnp.exp(scores - new)
                rescale = jnp.exp(old - new)
                top[h, :, columns] = new
                total[h, :, columns] = total[h, :, columns] * rescale + jnp.sum(
                    weights, axis=0, keepdims=True
                )
                acc[h, :, columns] = acc[h, :, columns] * rescale + jnp.dot(
                    v_t[...], weights.astype(jnp.bfloat16), preferred_element_type=jnp.float32
                )
            return carry

        lax.fori_loop(0, heads, head, 0)

    def forward(s, d, c):
        slot = 2 * s - 1 + d
        return ring_copy(slot, jnp.minimum(slot + 2, 2 * steps - 1), d, c)

    def arrived(slot, c):
        ring_copy(slot, slot, 0, c).wait_recv()

    def always(d, c):
        return (c < n_tp // 2) == (d == 0)

    def half_step(u, carry):
        s = u // 2 + 1
        for phase in range(2):

            @pl.when(jnp.logical_and(u < 2 * steps - 2, u % 2 == phase))
            def _():
                for c in (2 * phase, 2 * phase + 1):
                    for d in range(2):
                        arrived(2 * s - 1 + d, c)
                        if always(d, c):
                            forward(s, d, c).start()
                        else:

                            @pl.when(s < steps - 1)
                            def _():
                                forward(s, d, c).start()

            @pl.when(u == 2 * steps - 2 + phase)
            def _():
                arrived(2 * steps - 1, phase)
                arrived(2 * steps - 1, 2 + phase)

        @pl.when(u == 6)
        def _():
            w_right.wait_recv()
            w_right_on.start()
            w_left.wait_recv()
            w_left_on.start()

        fold(blocks.at[u])
        return carry

    lax.fori_loop(0, 2 * steps, half_step, 0)

    for h in range(heads):
        one = acc[h, :, :n_query] / total[h, :, :n_query]
        two = acc[h, :, n_query:] / total[h, :, n_query:]
        differ = one - lam[h] * two
        scale = lax.rsqrt(jnp.mean(differ * differ, axis=0, keepdims=True) + EPSILON)
        normed = differ * scale * head_gain[...] * HEAD_SCALE
        att[:, h * width : (h + 1) * width] = normed.T.astype(jnp.bfloat16)

    slot_of = {1: 2, 2: 3, 3: 1}
    sends = []
    for k in (1, 2, 3):
        span = pl.ds(slot_of[k] * own_rows, own_rows)
        sends.append(
            remote(att.at[span], got.at[k - 1], att_s.at[k - 1], att_r.at[k - 1], tp_peers[k - 1])
        )
    for copy in sends:
        copy.start()
    w_right_on.wait_recv()
    w_left_on.wait_recv()
    for copy in sends:
        copy.wait_recv()
    n_columns = latent.shape[1]
    step = 512
    for j in range(n_columns // step):
        columns = slice(j * step, (j + 1) * step)
        mixed = jnp.dot(att[:own_rows, :], w_own[:, columns], preferred_element_type=jnp.float32)
        for k in range(3):
            mixed += jnp.dot(got[k], w_far[k, :, columns], preferred_element_type=jnp.float32)
        out[:, columns] = (
            latent[:, columns].astype(jnp.float32) + mod[2:3, columns] * mixed
        ).astype(out.dtype)

    for copy in far_copies + near_copies + tp_copies + to_right + to_left + sends:
        copy.wait_send()
    for copy in [onward_right, onward_left, w_right, w_left, w_right_on, w_left_on]:
        copy.wait_send()
    for c in range(n_tp):
        for d in range(2):
            ring_copy(0, 1 + d, d, c).wait_send()

    def drain(s, carry):
        for c in range(n_tp):
            for d in range(2):
                if always(d, c):
                    forward(s, d, c).wait_send()
                else:

                    @pl.when(s < steps - 1)
                    def _():
                        forward(s, d, c).wait_send()

        return carry

    lax.fori_loop(1, steps, drain, 0)


def fused(n_sp, n_tp, lift, part, latent, context, norm_gain, w_query, w_key, w_value, lam, head_gain, w_out):
    dma = pltpu.SemaphoreType.DMA
    vmem = pl.BlockSpec(memory_space=pltpu.VMEM)
    anywhere = pl.BlockSpec(memory_space=pl.ANY)
    heads, width = lam.shape[0], head_gain.shape[0]
    own_rows, model = latent.shape
    n_query = n_tp * own_rows
    length = n_query + context.shape[0]
    bf16, f32 = jnp.bfloat16, jnp.float32
    return pl.pallas_call(
        functools.partial(fused_kernel, n_sp, n_tp, lift),
        out_shape=jax.ShapeDtypeStruct(latent.shape, latent.dtype),
        in_specs=[vmem] * 4
        + [anywhere] * 3
        + [pl.BlockSpec(memory_space=pltpu.SMEM), vmem, anywhere],
        out_specs=vmem,
        scratch_shapes=[
            pltpu.VMEM((3,) + part.shape, f32),
            pltpu.VMEM((3,) + part.shape, f32),
            pltpu.VMEM(part.shape, f32),
            pltpu.VMEM((part.shape[0], model), f32),
            pltpu.VMEM((3, own_rows, model), bf16),
            pltpu.VMEM((3,) + w_key.shape, bf16),
            pltpu.VMEM((model, 2 * heads * width), bf16),
            pltpu.VMEM((model, heads * width), bf16),
            pltpu.VMEM(w_out.shape, bf16),
            pltpu.VMEM((3,) + w_out.shape, bf16),
            pltpu.VMEM((own_rows + context.shape[0], model), bf16),
            pltpu.VMEM((n_query, heads * width), bf16),
            pltpu.VMEM((n_sp, length, 2 * heads * width), bf16),
            pltpu.VMEM((heads * width, 2 * n_query), bf16),
            pltpu.VMEM((heads, width, 2 * n_query), f32),
            pltpu.VMEM((heads, 1, 2 * n_query), f32),
            pltpu.VMEM((heads, 1, 2 * n_query), f32),
            pltpu.VMEM((width, length), bf16),
            pltpu.VMEM((n_query, heads * width), bf16),
            pltpu.VMEM((3, own_rows, heads * width), bf16),
            dma((3,)),
            dma((3,)),
            dma((3,)),
            dma((3,)),
            dma((3,)),
            dma((3,)),
            dma((8,)),
            dma((8,)),
            dma((4,)),
            dma((n_sp, 2, n_tp)),
            dma((n_sp, n_tp)),
            dma((4,)),
            dma((4,)),
            dma((3,)),
            dma((3,)),
        ],
        compiler_params=pltpu.CompilerParams(
            collective_id=0, has_side_effects=True, vmem_limit_bytes=60 * 1024 * 1024
        ),
        name="fused",
    )(part, latent, context, norm_gain, w_query, w_key, w_value, lam, head_gain, w_out)


def on_device(
    latent, cond, cond_ctx, context, w_mod, norm_gain, w_query, w_key, w_value, lam, head_gain, w_out
):
    n_sp, n_tp = lax.axis_size("sp"), lax.axis_size("tp")
    lift = math.log(TOK_DEV / (4 * CTX_DEV))
    cond_rows = jnp.concatenate(
        [cond.astype(jnp.float32), cond_ctx.astype(jnp.float32)[None]], axis=0
    )
    partial_mod = jnp.einsum(
        "sd,jde->sje",
        jax.nn.silu(cond_rows),
        w_mod.astype(jnp.float32),
        precision=lax.Precision.HIGHEST,
    )
    columns = w_mod.shape[2]
    part = jnp.concatenate(
        [partial_mod.reshape(6, columns), jnp.zeros((2, columns), jnp.float32)], axis=0
    )
    updated = fused(
        n_sp,
        n_tp,
        lift,
        part,
        latent[0],
        context[0],
        norm_gain[None],
        w_query,
        w_key,
        w_value,
        lam,
        head_gain[:, None],
        w_out.reshape(-1, w_out.shape[2]),
    )
    return updated[None]


def solution(mesh):
    return jax.shard_map(
        on_device,
        mesh=mesh,
        in_specs=(
            P(("grp", "dp"), ("sp", "tp"), None),
            P(("grp", "dp"), "sp"),
            P("sp"),
            P(("grp", "dp"), "sp", None),
            P(None, "sp", "tp"),
            P(),
            P(None, "tp", None),
            P(None, "tp", None),
            P(None, "tp", None),
            P("tp"),
            P(),
            P("tp", None, None),
        ),
        out_specs=P(("grp", "dp"), ("sp", "tp"), None),
        check_vma=False,
    )
```

time: 202 us -> 180 us (0.89)
  Pallas kernels: 185 us -> 175 us
  other arithmetic: 7.31 us -> 0 us
  matrix products: 4.47 us -> 0.27 us
    pallas_call x2 -> x1, Pallas kernels: 185 us -> 175 us  [fused(): pl.pallas_call(functools.partial(fused_kernel, n_sp, n_tp, lift), out_sha...]
    dot_general x3 -> x0, matrix products: 3.53 us -> none  [the longest x1 1.75 us: on_device(): lax.dot_general(flat(w_query), normed, (((0,), (1,)), ((), ())), preferre...]
    reduce_sum x2 -> x0, other arithmetic: 2.47 us -> none  [modulated_norm(): jnp.mean(values_f * values_f, axis=-1, keepdims=True) + EPSILON]
    convert_element_type x3 -> x0, other arithmetic: 2.18 us -> none  [modulated_norm(): return (normed * norm_gain * (1.0 + scale) + shift).astype(jnp.bfloat16)]
where the time goes in v2:
time: 180 us
  Pallas kernels  175 us (97%)
  local copies, waits for them, and re-layouts  4.39 us (2%)
    pallas_call x1, Pallas kernels, fused(): pl.pallas_call(functools.partial(fused_kernel, n_sp, n_tp, lift), out_sha...  175 us

profile of v2, /device:TPU:40, one launch (start us, length us, event | category | flops | bytes accessed | tf_op | source)
XLA Modules:
  0.0 179.8 jit_solution(3451900302482135988)
XLA Ops:
  0.0 0.0 copy-start
  0.0 0.0 copy-start.1
  0.0 0.0 copy-start.2
  0.0 1.0 copy-done
  1.0 0.0 copy-done.1
  1.0 0.0 copy-done.2
  1.0 0.3 fusion.3
  1.3 0.0 copy-start.3
  1.3 0.6 concatenate.11.part
  1.9 0.0 copy-done.3
  2.0 0.7 copy.16.head_gain
  2.7 175.1 %fused.1 = bf16[160,2048]{1,0:T(8,128)(2,1)} custom-call(f32[8,512]{1,0:T(8,128)} %concatenate.11.part, bf16[160,2048]{1,0:T(8,128)(2,1)} %bitcast.13, bf16[32,2048]{1,0:T(8,128)(2,1)} %bitcast.14, f32[1,2048]{1,0:T(1,128)} %bitcast.15, bf16[2048,2,128]{2,1,0:T(2,128)(2,1)} %w_query.1, bf16[2048,2,128]{2,1,0:T(2,128)(2,1)} %w_key.1, ...), custom_call_target="tpu_custom_call" | custom-call | tf_op jit(solution)/shard_map/fused/pallas_call | solution.py:365
  177.8 2.0 %copy.18 = bf16[1,160,2048]{2,1,0:T(8,128)(2,1)} copy(bf16[1,160,2048]{2,1,0:T(8,128)(2,1)} %bitcast.11) | data formatting | bytes 1310720
  (2 shorter events, 0.0 us)
Async XLA Ops:
  0.0 1.0 copy-start
  0.0 1.0 copy-start.1
  0.0 1.0 copy-start.2
  1.3 0.7 copy-start.3

commit v3 on v2

--- a/solution.py
+++ b/solution.py
@@ -28,19 +28,12 @@
     )
 
 
-def greet(peers):
-    barrier = pltpu.get_barrier_semaphore()
-    for peer in peers:
-        pl.semaphore_signal(barrier, inc=1, device_id=peer, device_id_type=MESH)
-    pl.semaphore_wait(barrier, len(peers))
-
-
 def fused_kernel(
     n_sp, n_tp, lift,
-    part, latent, context, norm_gain, w_query, w_key, w_value, lam, head_gain, w_out, out,
-    far, near, sums, mod, rows, w_raw, w_kv, w_q, w_own, w_far, tokens, queries,
+    latent_in, cond, cond_ctx, context_in, w_mod, norm_gain, w_query, w_key, w_value, lam, head_gain, w_out, out,
+    latent, context, w_mods, part, parts, mod, rows, w_raw, w_kv, w_q, w_own, w_far, tokens, queries,
     blocks, q_wide, acc, top, total, v_t, att, got,
-    far_s, far_r, near_s, near_r, tp_s, tp_r, lat_s, lat_r, load_s, ring_s, ring_r, w_s, w_r, att_s, att_r,
+    part_s, part_r, tp_s, tp_r, lat_s, lat_r, load_s, ring_s, ring_r, w_s, w_r, att_s, att_r,
 ):
     z = lax.axis_index("sp")
     x = lax.axis_index("tp")
@@ -60,25 +53,66 @@
     def tp_at(offset):
         return {"tp": lax.rem(x + offset, n_tp)}
 
-    quarter = n_sp // 4
-    far_peers = [sp_at(quarter * k) for k in (1, 2, 3)]
-    near_peers = [sp_at(1), sp_at(-1), sp_at(2)]
     tp_peers = [tp_at(k) for k in (1, 2, 3)]
     right, left = tp_peers[0], tp_peers[2]
     ring_peers = [sp_at(1), sp_at(-1)]
 
-    raw = [w_key, w_value, w_query]
-    raw_loads = [pltpu.make_async_copy(raw[k], w_raw.at[k], load_s.at[k]) for k in range(3)]
-    out_load = pltpu.make_async_copy(w_out, w_own, load_s.at[3])
-    for copy in raw_loads + [out_load]:
+    loads = [
+        pltpu.make_async_copy(source, target, load_s.at[k])
+        for k, (source, target) in enumerate(
+            (
+                (w_mod, w_mods),
+                (latent_in, latent),
+                (context_in, context),
+                (w_key, w_raw.at[0]),
+                (w_value, w_raw.at[1]),
+                (w_query, w_raw.at[2]),
+                (w_out, w_own),
+            )
+        )
+    ]
+    mod_load, latent_load, context_load, out_load = loads[0], loads[1], loads[2], loads[6]
+    raw_loads = loads[3:6]
+    for copy in loads:
         copy.start()
-    greet(far_peers + near_peers + [sp_at(-2)] + tp_peers)
-
-    far_copies = [
-        remote(part, far.at[k], far_s.at[k], far_r.at[k], far_peers[k]) for k in range(3)
+    everyone = [sp_at(k) for k in range(1, n_sp)] + tp_peers
+    barrier = pltpu.get_barrier_semaphore()
+    for peer in everyone:
+        pl.semaphore_signal(barrier, inc=1, device_id=peer, device_id_type=MESH)
+
+    def gated(ref):
+        values = ref[...].astype(jnp.float32)
+        return values * jax.nn.sigmoid(values)
+
+    row = lax.broadcasted_iota(jnp.int32, (16, cond.shape[1]), 0)
+    silu = jnp.where(row % 2 == 0, gated(cond), gated(cond_ctx))
+    high = silu.astype(jnp.bfloat16)
+    rest = silu - high.astype(jnp.float32)
+    middle = rest.astype(jnp.bfloat16)
+    low = (rest - middle.astype(jnp.float32)).astype(jnp.bfloat16)
+    split = jnp.where(
+        row < 2,
+        high.astype(jnp.float32),
+        jnp.where(
+            row < 4, middle.astype(jnp.float32), jnp.where(row < 6, low.astype(jnp.float32), 0.0)
+        ),
+    ).astype(jnp.bfloat16)
+    part[...] = jnp.zeros_like(part)
+    mod_load.wait()
+    for j in range(w_mods.shape[0]):
+        thirds = jnp.dot(split, w_mods[j], preferred_element_type=jnp.float32)
+        both = thirds[4:6] + thirds[2:4] + thirds[0:2]
+        part[j : j + 1, :] = both[0:1]
+        part[3 + j : 4 + j, :] = both[1:2]
+    pl.semaphore_wait(barrier, len(everyone))
+
+    part_copies = [
+        remote(part, parts.at[k - 1], part_s.at[k - 1], part_r.at[k - 1], everyone[k - 1])
+        for k in range(1, n_sp)
     ]
-    for copy in far_copies:
-        copy.start()
+    for k in sorted(range(1, n_sp), key=lambda k: abs(k - steps)):
+        part_copies[k - 1].start()
+    latent_load.wait()
 
     half = own_rows // 2
     piece = 48
@@ -114,19 +148,11 @@
             column = (k * heads + h) * width
             w_kv[:, column : column + width] = w_raw[k, :, h, :]
 
-    for copy in far_copies:
+    for copy in part_copies:
         copy.wait_recv()
-    sums[...] = part[...] + far[0] + far[1] + far[2]
-    near_copies = [
-        remote(sums, near.at[k], near_s.at[k], near_r.at[k], near_peers[k]) for k in range(3)
-    ]
-    for copy in near_copies:
-        copy.start()
-    raw_loads[2].wait()
-    for h in range(heads):
-        w_q[:, h * width : (h + 1) * width] = w_raw[2, :, h, :]
-    for copy in near_copies:
-        copy.wait_recv()
+    whole = part[...]
+    for k in range(1, n_sp):
+        whole = whole + parts[k - 1]
     columns = part.shape[1]
 
     def mod_of(owner):
@@ -134,7 +160,7 @@
         return mod.at[:, span]
 
     mine = pl.ds(pl.multiple_of(x * columns, columns), columns)
-    mod[:, mine] = sums[...] + near[0] + near[1] + near[2]
+    mod[:, mine] = whole
     tp_copies = [
         remote(mod_of(x), mod_of(x), tp_s.at[k], tp_r.at[k], tp_peers[k]) for k in range(3)
     ]
@@ -146,6 +172,10 @@
     onward_right.start()
     to_left[0].wait_recv()
     onward_left.start()
+    raw_loads[2].wait()
+    for h in range(heads):
+        w_q[:, h * width : (h + 1) * width] = w_raw[2, :, h, :]
+    context_load.wait()
     for k in range(3):
         theirs = mod_of(lax.rem(x + n_tp - 1 - k, n_tp))
         remote(theirs, theirs, tp_s.at[k], tp_r.at[k], tp_peers[k]).wait_recv()
@@ -220,7 +250,7 @@
                 half_width ** (-0.5)
             )
 
-    def fold(block):
+    def fold(block, after=None):
         def head(h, carry):
             base = pl.multiple_of(h * width, width)
             keys = block[:, pl.ds(base, width)]
@@ -249,6 +279,8 @@
                 acc[h, :, columns] = acc[h, :, columns] * rescale + jnp.dot(
                     v_t[...], weights.astype(jnp.bfloat16), preferred_element_type=jnp.float32
                 )
+            if after is not None:
+                after(h, base)
             return carry
 
         lax.fori_loop(0, heads, head, 0)
@@ -280,10 +312,10 @@
                             def _():
                                 forward(s, d, c).start()
 
-            @pl.when(u == 2 * steps - 2 + phase)
-            def _():
-                arrived(2 * steps - 1, phase)
-                arrived(2 * steps - 1, 2 + phase)
+        @pl.when(u == 2 * steps - 2)
+        def _():
+            arrived(2 * steps - 1, 0)
+            arrived(2 * steps - 1, 2)
 
         @pl.when(u == 6)
         def _():
@@ -295,25 +327,35 @@
         fold(blocks.at[u])
         return carry
 
-    lax.fori_loop(0, 2 * steps, half_step, 0)
-
-    for h in range(heads):
+    lax.fori_loop(0, 2 * steps - 1, half_step, 0)
+
+    slot_of = {1: 2, 2: 3, 3: 1}
+
+    def send_head(h, base, k):
+        span = pl.ds(slot_of[k] * own_rows, own_rows)
+        lanes = pl.ds(base, width)
+        return remote(
+            att.at[span, lanes],
+            got.at[k - 1, :, lanes],
+            att_s.at[k - 1, h],
+            att_r.at[k - 1, h],
+            tp_peers[k - 1],
+        )
+
+    def finish(h, base):
         one = acc[h, :, :n_query] / total[h, :, :n_query]
         two = acc[h, :, n_query:] / total[h, :, n_query:]
         differ = one - lam[h] * two
         scale = lax.rsqrt(jnp.mean(differ * differ, axis=0, keepdims=True) + EPSILON)
         normed = differ * scale * head_gain[...] * HEAD_SCALE
-        att[:, h * width : (h + 1) * width] = normed.T.astype(jnp.bfloat16)
-
-    slot_of = {1: 2, 2: 3, 3: 1}
-    sends = []
-    for k in (1, 2, 3):
-        span = pl.ds(slot_of[k] * own_rows, own_rows)
-        sends.append(
-            remote(att.at[span], got.at[k - 1], att_s.at[k - 1], att_r.at[k - 1], tp_peers[k - 1])
-        )
-    for copy in sends:
-        copy.start()
+        att[:, pl.ds(base, width)] = normed.T.astype(jnp.bfloat16)
+        for k in (2, 1, 3):
+            send_head(h, base, k).start()
+
+    arrived(2 * steps - 1, 1)
+    arrived(2 * steps - 1, 3)
+    fold(blocks.at[2 * steps - 1], finish)
+    sends = [send_head(h, h * width, k) for h in range(heads) for k in (2, 1, 3)]
     w_right_on.wait_recv()
     w_left_on.wait_recv()
     for copy in sends:
@@ -329,7 +371,7 @@
             latent[:, columns].astype(jnp.float32) + mod[2:3, columns] * mixed
         ).astype(out.dtype)
 
-    for copy in far_copies + near_copies + tp_copies + to_right + to_left + sends:
+    for copy in part_copies + tp_copies + to_right + to_left + sends:
         copy.wait_send()
     for copy in [onward_right, onward_left, w_right, w_left, w_right_on, w_left_on]:
         copy.wait_send()
@@ -353,7 +395,7 @@
     lax.fori_loop(1, steps, drain, 0)
 
 
-def fused(n_sp, n_tp, lift, part, latent, context, norm_gain, w_query, w_key, w_value, lam, head_gain, w_out):
+def fused(n_sp, n_tp, lift, latent, cond, cond_ctx, context, w_mod, norm_gain, w_query, w_key, w_value, lam, head_gain, w_out):
     dma = pltpu.SemaphoreType.DMA
     vmem = pl.BlockSpec(memory_space=pltpu.VMEM)
     anywhere = pl.BlockSpec(memory_space=pl.ANY)
@@ -365,15 +407,17 @@
     return pl.pallas_call(
         functools.partial(fused_kernel, n_sp, n_tp, lift),
         out_shape=jax.ShapeDtypeStruct(latent.shape, latent.dtype),
-        in_specs=[vmem] * 4
+        in_specs=[anywhere, vmem, vmem, anywhere, anywhere, vmem]
         + [anywhere] * 3
         + [pl.BlockSpec(memory_space=pltpu.SMEM), vmem, anywhere],
         out_specs=vmem,
         scratch_shapes=[
-            pltpu.VMEM((3,) + part.shape, f32),
-            pltpu.VMEM((3,) + part.shape, f32),
-            pltpu.VMEM(part.shape, f32),
-            pltpu.VMEM((part.shape[0], model), f32),
+            pltpu.VMEM(latent.shape, bf16),
+            pltpu.VMEM(context.shape, bf16),
+            pltpu.VMEM(w_mod.shape, bf16),
+            pltpu.VMEM((8, w_mod.shape[2]), f32),
+            pltpu.VMEM((n_sp - 1, 8, w_mod.shape[2]), f32),
+            pltpu.VMEM((8, model), f32),
             pltpu.VMEM((3, own_rows, model), bf16),
             pltpu.VMEM((3,) + w_key.shape, bf16),
             pltpu.VMEM((model, 2 * heads * width), bf16),
@@ -390,27 +434,25 @@
             pltpu.VMEM((width, length), bf16),
             pltpu.VMEM((n_query, heads * width), bf16),
             pltpu.VMEM((3, own_rows, heads * width), bf16),
-            dma((3,)),
-            dma((3,)),
-            dma((3,)),
-            dma((3,)),
+            dma((n_sp - 1,)),
+            dma((n_sp - 1,)),
             dma((3,)),
             dma((3,)),
             dma((8,)),
             dma((8,)),
-            dma((4,)),
+            dma((7,)),
             dma((n_sp, 2, n_tp)),
             dma((n_sp, n_tp)),
             dma((4,)),
             dma((4,)),
-            dma((3,)),
-            dma((3,)),
+            dma((3, heads)),
+            dma((3, heads)),
         ],
         compiler_params=pltpu.CompilerParams(
             collective_id=0, has_side_effects=True, vmem_limit_bytes=60 * 1024 * 1024
         ),
         name="fused",
-    )(part, latent, context, norm_gain, w_query, w_key, w_value, lam, head_gain, w_out)
+    )(latent, cond, cond_ctx, context, w_mod, norm_gain, w_query, w_key, w_value, lam, head_gain, w_out)
 
 
 def on_device(
@@ -418,26 +460,15 @@
 ):
     n_sp, n_tp = lax.axis_size("sp"), lax.axis_size("tp")
     lift = math.log(TOK_DEV / (4 * CTX_DEV))
-    cond_rows = jnp.concatenate(
-        [cond.astype(jnp.float32), cond_ctx.astype(jnp.float32)[None]], axis=0
-    )
-    partial_mod = jnp.einsum(
-        "sd,jde->sje",
-        jax.nn.silu(cond_rows),
-        w_mod.astype(jnp.float32),
-        precision=lax.Precision.HIGHEST,
-    )
-    columns = w_mod.shape[2]
-    part = jnp.concatenate(
-        [partial_mod.reshape(6, columns), jnp.zeros((2, columns), jnp.float32)], axis=0
-    )
     updated = fused(
         n_sp,
         n_tp,
         lift,
-        part,
         latent[0],
+        cond,
+        cond_ctx[None],
         context[0],
+        w_mod,
         norm_gain[None],
         w_query,
         w_key,

time: 180 us -> 178 us (0.989)
  no operation moved by 1% of the time
where the time goes in v3:
time: 178 us
  Pallas kernels  175 us (98%)
  local copies, waits for them, and re-layouts  3.38 us (2%)
    pallas_call x1, Pallas kernels, fused(): pl.pallas_call(functools.partial(fused_kernel, n_sp, n_tp, lift), out_sha...  175 us

profile of v3, /device:TPU:40, one launch (start us, length us, event | category | flops | bytes accessed | tf_op | source)
XLA Modules:
  0.0 178.3 jit_solution(11651622374698593445)
XLA Ops:
  0.0 0.0 copy-start
  0.0 0.7 copy-done
  0.7 0.7 copy.13.head_gain
  1.4 174.9 %fused.1 = bf16[160,2048]{1,0:T(8,128)(2,1)} custom-call(bf16[160,2048]{1,0:T(8,128)(2,1)} %bitcast.9, bf16[1,128]{1,0:T(2,128)(2,1)} %cond.1, bf16[1,128]{1,0:T(2,128)(2,1)} %bitcast.13, bf16[32,2048]{1,0:T(8,128)(2,1)} %bitcast.10, bf16[3,128,512]{2,1,0:T(8,128)(2,1)} %w_mod.1, f32[1,2048]{1,0:T(1,128)} %bitcast.11, bf16[2048,2,128]{2,1,0:T(2,128)(2,1)} %w_query.1, ...), custom_call_target="tpu_custom_call" | custom-call | tf_op jit(solution)/shard_map/fused/pallas_call | solution.py:407
  176.3 2.0 %copy.15 = bf16[1,160,2048]{2,1,0:T(8,128)(2,1)} copy(bf16[1,160,2048]{2,1,0:T(8,128)(2,1)} %bitcast.7) | data formatting | bytes 1310720
Async XLA Ops:
  0.0 0.7 copy-start

commit v4 on v3

--- a/solution.py
+++ b/solution.py
@@ -31,9 +31,9 @@
 def fused_kernel(
     n_sp, n_tp, lift,
     latent_in, cond, cond_ctx, context_in, w_mod, norm_gain, w_query, w_key, w_value, lam, head_gain, w_out, out,
-    latent, context, w_mods, part, parts, mod, rows, w_raw, w_kv, w_q, w_own, w_far, tokens, queries,
+    latent, context, w_mods, part, parts, gate, gates, mod, whole_gate, rows, w_raw, w_kv, w_q, w_own, w_far, tokens, queries,
     blocks, q_wide, acc, top, total, v_t, att, got,
-    part_s, part_r, tp_s, tp_r, lat_s, lat_r, load_s, ring_s, ring_r, w_s, w_r, att_s, att_r,
+    part_s, part_r, gate_s, gate_r, tp_s, tp_r, gate_tp_s, gate_tp_r, lat_s, lat_r, load_s, ring_s, ring_r, w_s, w_r, att_s, att_r,
 ):
     z = lax.axis_index("sp")
     x = lax.axis_index("tp")
@@ -97,21 +97,28 @@
             row < 4, middle.astype(jnp.float32), jnp.where(row < 6, low.astype(jnp.float32), 0.0)
         ),
     ).astype(jnp.bfloat16)
-    part[...] = jnp.zeros_like(part)
+    columns = w_mods.shape[2]
+    middle_column = columns // 2
     mod_load.wait()
     for j in range(w_mods.shape[0]):
         thirds = jnp.dot(split, w_mods[j], preferred_element_type=jnp.float32)
         both = thirds[4:6] + thirds[2:4] + thirds[0:2]
-        part[j : j + 1, :] = both[0:1]
-        part[3 + j : 4 + j, :] = both[1:2]
+        if j == 2:
+            gate[...] = both[0:1]
+        else:
+            for of_ctx in range(2):
+                at = 2 * of_ctx + j
+                part[at : at + 1, :] = both[of_ctx : of_ctx + 1, :middle_column]
+                part[4 + at : 5 + at, :] = both[of_ctx : of_ctx + 1, middle_column:]
     pl.semaphore_wait(barrier, len(everyone))
 
-    part_copies = [
-        remote(part, parts.at[k - 1], part_s.at[k - 1], part_r.at[k - 1], everyone[k - 1])
-        for k in range(1, n_sp)
-    ]
-    for k in sorted(range(1, n_sp), key=lambda k: abs(k - steps)):
-        part_copies[k - 1].start()
+    far_first = sorted(range(n_sp - 1), key=lambda k: abs(k + 1 - steps))
+    part_copies = [remote(part, parts.at[k], part_s, part_r, everyone[k]) for k in far_first]
+    gate_copies = [remote(gate, gates.at[k], gate_s, gate_r, everyone[k]) for k in far_first]
+    all_parts = remote(parts, parts, part_s, part_r, everyone[0])
+    all_gates = remote(gates, gates, gate_s, gate_r, everyone[0])
+    for copy in part_copies + gate_copies:
+        copy.start()
     latent_load.wait()
 
     half = own_rows // 2
@@ -148,19 +155,19 @@
             column = (k * heads + h) * width
             w_kv[:, column : column + width] = w_raw[k, :, h, :]
 
-    for copy in part_copies:
-        copy.wait_recv()
+    all_parts.wait_recv()
     whole = part[...]
-    for k in range(1, n_sp):
-        whole = whole + parts[k - 1]
-    columns = part.shape[1]
+    for k in range(n_sp - 1):
+        whole = whole + parts[k]
 
     def mod_of(owner):
         span = pl.ds(pl.multiple_of(owner * columns, columns), columns)
         return mod.at[:, span]
 
     mine = pl.ds(pl.multiple_of(x * columns, columns), columns)
-    mod[:, mine] = whole
+    at_middle = pl.multiple_of(x * columns + middle_column, middle_column)
+    mod[:, pl.ds(pl.multiple_of(x * columns, columns), middle_column)] = whole[:4]
+    mod[:, pl.ds(at_middle, middle_column)] = whole[4:]
     tp_copies = [
         remote(mod_of(x), mod_of(x), tp_s.at[k], tp_r.at[k], tp_peers[k]) for k in range(3)
     ]
@@ -195,12 +202,12 @@
 
         lax.fori_loop(0, count // group, some, 0, unroll=2)
 
-    def ring_copy(slot, target, d, c):
+    def ring_copy(slot, target, d, c, turn=0):
         span = pl.ds(starts[c], sizes[c])
         return remote(
             blocks.at[slot, span],
             blocks.at[target, span],
-            ring_s.at[slot, d, c],
+            ring_s.at[turn, d, c],
             ring_r.at[target, c],
             ring_peers[d],
         )
@@ -217,7 +224,7 @@
             ring_copy(0, 1 + d, d, c).start()
 
     norm(latent, 0, own_rows, 0)
-    norm(context, own_rows, n_ctx, 3)
+    norm(context, own_rows, n_ctx, 2)
     project(0)
     for k in (1, 2):
         to_right[k].wait_recv()
@@ -232,6 +239,22 @@
     norm(rows.at[2], 0, own_rows, 0)
     project(3)
 
+    all_gates.wait_recv()
+    gate_sum = gate[...]
+    for k in range(n_sp - 1):
+        gate_sum = gate_sum + gates[k]
+    whole_gate[:, mine] = gate_sum
+
+    def gate_of(owner):
+        return whole_gate.at[:, pl.ds(pl.multiple_of(owner * columns, columns), columns)]
+
+    gate_tp_copies = [
+        remote(gate_of(x), gate_of(x), gate_tp_s.at[k], gate_tp_r.at[k], tp_peers[k])
+        for k in range(3)
+    ]
+    for copy in gate_tp_copies:
+        copy.start()
+
     w_rows = w_own.shape[0]
     upper, lower = pl.ds(0, w_rows // 2), pl.ds(w_rows // 2, w_rows // 2)
     w_right = remote(w_own, w_far.at[0], w_s.at[0], w_r.at[0], right)
@@ -250,24 +273,31 @@
                 half_width ** (-0.5)
             )
 
-    def fold(block, after=None):
+    half_row = starts[n_tp // 2]
+    spans = [(0, half_row), (half_row, length)]
+
+    def fold(block, phase, after=None):
+        begin, end = spans[phase]
+        count = end - begin
+
         def head(h, carry):
             base = pl.multiple_of(h * width, width)
-            keys = block[:, pl.ds(base, width)]
-            v_t[...] = block[:, pl.ds(pl.multiple_of(heads * width + base, width), width)].T
+            keys = block[begin:end, pl.ds(base, width)]
+            v_t[:, :count] = block[begin:end, pl.ds(pl.multiple_of(heads * width + base, width), width)].T
             for j in range(tiles):
                 columns = slice(j * QTILE, (j + 1) * QTILE)
                 scores = jnp.dot(
                     keys, q_wide[pl.ds(base, width), columns], preferred_element_type=jnp.float32
                 )
-                scores = jnp.concatenate(
-                    [
-                        scores[:own_rows],
-                        scores[own_rows : own_rows + n_ctx] + lift,
-                        scores[own_rows + n_ctx :],
-                    ],
-                    axis=0,
-                )
+                if phase == 0:
+                    scores = jnp.concatenate(
+                        [
+                            scores[:own_rows],
+                            scores[own_rows : own_rows + n_ctx] + lift,
+                            scores[own_rows + n_ctx :],
+                        ],
+                        axis=0,
+                    )
                 old = top[h, :, columns]
                 new = jnp.maximum(old, jnp.max(scores, axis=0, keepdims=True))
                 weights = jnp.exp(scores - new)
@@ -277,7 +307,7 @@
                     weights, axis=0, keepdims=True
                 )
                 acc[h, :, columns] = acc[h, :, columns] * rescale + jnp.dot(
-                    v_t[...], weights.astype(jnp.bfloat16), preferred_element_type=jnp.float32
+                    v_t[:, :count], weights.astype(jnp.bfloat16), preferred_element_type=jnp.float32
                 )
             if after is not None:
                 after(h, base)
@@ -287,13 +317,20 @@
 
     def forward(s, d, c):
         slot = 2 * s - 1 + d
-        return ring_copy(slot, jnp.minimum(slot + 2, 2 * steps - 1), d, c)
+        return ring_copy(slot, jnp.minimum(slot + 2, 2 * steps - 1), d, c, lax.rem(s, 2))
+
+    def send_on(s, d, c):
+        @pl.when(s >= 2)
+        def _():
+            ring_copy(0, 1 + d, d, c, lax.rem(s, 2)).wait_send()
+
+        forward(s, d, c).start()
 
     def arrived(slot, c):
         ring_copy(slot, slot, 0, c).wait_recv()
 
     def always(d, c):
-        return (c < n_tp // 2) == (d == 0)
+        return c % 2 == d
 
     def half_step(u, carry):
         s = u // 2 + 1
@@ -305,17 +342,17 @@
                     for d in range(2):
                         arrived(2 * s - 1 + d, c)
                         if always(d, c):
-                            forward(s, d, c).start()
+                            send_on(s, d, c)
                         else:
 
                             @pl.when(s < steps - 1)
                             def _():
-                                forward(s, d, c).start()
+                                send_on(s, d, c)
 
         @pl.when(u == 2 * steps - 2)
         def _():
             arrived(2 * steps - 1, 0)
-            arrived(2 * steps - 1, 2)
+            arrived(2 * steps - 1, 1)
 
         @pl.when(u == 6)
         def _():
@@ -324,7 +361,26 @@
             w_left.wait_recv()
             w_left_on.start()
 
-        fold(blocks.at[u])
+        for phase in range(2):
+
+            @pl.when(u % 2 == phase)
+            def _():
+                def one_half(k, carry):
+                    wanted = jnp.logical_or(
+                        k == 1,
+                        jnp.logical_or(
+                            jnp.logical_and(k == 0, s == 1), jnp.logical_and(k == 2, s < steps)
+                        ),
+                    )
+
+                    @pl.when(wanted)
+                    def _():
+                        fold(blocks.at[2 * s - 2 + k], phase)
+
+                    return carry
+
+                lax.fori_loop(0, 3, one_half, 0)
+
         return carry
 
     lax.fori_loop(0, 2 * steps - 1, half_step, 0)
@@ -352,14 +408,17 @@
         for k in (2, 1, 3):
             send_head(h, base, k).start()
 
-    arrived(2 * steps - 1, 1)
+    arrived(2 * steps - 1, 2)
     arrived(2 * steps - 1, 3)
-    fold(blocks.at[2 * steps - 1], finish)
+    fold(blocks.at[2 * steps - 1], 1, finish)
     sends = [send_head(h, h * width, k) for h in range(heads) for k in (2, 1, 3)]
     w_right_on.wait_recv()
     w_left_on.wait_recv()
     for copy in sends:
         copy.wait_recv()
+    for k in range(3):
+        theirs = gate_of(lax.rem(x + n_tp - 1 - k, n_tp))
+        remote(theirs, theirs, gate_tp_s.at[k], gate_tp_r.at[k], tp_peers[k]).wait_recv()
     n_columns = latent.shape[1]
     step = 512
     for j in range(n_columns // step):
@@ -368,31 +427,19 @@
         for k in range(3):
             mixed += jnp.dot(got[k], w_far[k, :, columns], preferred_element_type=jnp.float32)
         out[:, columns] = (
-            latent[:, columns].astype(jnp.float32) + mod[2:3, columns] * mixed
+            latent[:, columns].astype(jnp.float32) + whole_gate[:, columns] * mixed
         ).astype(out.dtype)
 
-    for copy in part_copies + tp_copies + to_right + to_left + sends:
+    all_parts.wait_send()
+    all_gates.wait_send()
+    for copy in gate_tp_copies + tp_copies + to_right + to_left + sends:
         copy.wait_send()
     for copy in [onward_right, onward_left, w_right, w_left, w_right_on, w_left_on]:
         copy.wait_send()
-    for c in range(n_tp):
-        for d in range(2):
-            ring_copy(0, 1 + d, d, c).wait_send()
-
-    def drain(s, carry):
+    for turn in range(2):
         for c in range(n_tp):
             for d in range(2):
-                if always(d, c):
-                    forward(s, d, c).wait_send()
-                else:
-
-                    @pl.when(s < steps - 1)
-                    def _():
-                        forward(s, d, c).wait_send()
-
-        return carry
-
-    lax.fori_loop(1, steps, drain, 0)
+                ring_copy(0, 1 + d, d, c, turn).wait_send()
 
 
 def fused(n_sp, n_tp, lift, latent, cond, cond_ctx, context, w_mod, norm_gain, w_query, w_key, w_value, lam, head_gain, w_out):
@@ -415,9 +462,12 @@
             pltpu.VMEM(latent.shape, bf16),
             pltpu.VMEM(context.shape, bf16),
             pltpu.VMEM(w_mod.shape, bf16),
-            pltpu.VMEM((8, w_mod.shape[2]), f32),
-            pltpu.VMEM((n_sp - 1, 8, w_mod.shape[2]), f32),
-            pltpu.VMEM((8, model), f32),
+            pltpu.VMEM((8, w_mod.shape[2] // 2), f32),
+            pltpu.VMEM((n_sp - 1, 8, w_mod.shape[2] // 2), f32),
+            pltpu.VMEM((1, w_mod.shape[2]), f32),
+            pltpu.VMEM((n_sp - 1, 1, w_mod.shape[2]), f32),
+            pltpu.VMEM((4, model), f32),
+            pltpu.VMEM((1, model), f32),
             pltpu.VMEM((3, own_rows, model), bf16),
             pltpu.VMEM((3,) + w_key.shape, bf16),
             pltpu.VMEM((model, 2 * heads * width), bf16),
@@ -431,17 +481,21 @@
             pltpu.VMEM((heads, width, 2 * n_query), f32),
             pltpu.VMEM((heads, 1, 2 * n_query), f32),
             pltpu.VMEM((heads, 1, 2 * n_query), f32),
-            pltpu.VMEM((width, length), bf16),
+            pltpu.VMEM((width, 512), bf16),
             pltpu.VMEM((n_query, heads * width), bf16),
             pltpu.VMEM((3, own_rows, heads * width), bf16),
-            dma((n_sp - 1,)),
-            dma((n_sp - 1,)),
+            dma,
+            dma,
+            dma,
+            dma,
+            dma((3,)),
+            dma((3,)),
             dma((3,)),
             dma((3,)),
             dma((8,)),
             dma((8,)),
             dma((7,)),
-            dma((n_sp, 2, n_tp)),
+            dma((2, 2, n_tp)),
             dma((n_sp, n_tp)),
             dma((4,)),
             dma((4,)),

time: 178 us -> 175 us (0.983)
  Pallas kernels: 175 us -> 172 us
    pallas_call x1, Pallas kernels: 175 us -> 172 us  [fused(): pl.pallas_call(functools.partial(fused_kernel, n_sp, n_tp, lift), out_sha...]
where the time goes in v4:
time: 175 us
  Pallas kernels  172 us (98%)
  local copies, waits for them, and re-layouts  3.38 us (2%)
    pallas_call x1, Pallas kernels, fused(): pl.pallas_call(functools.partial(fused_kernel, n_sp, n_tp, lift), out_sha...  172 us

profile of v4, /device:TPU:40, one launch (start us, length us, event | category | flops | bytes accessed | tf_op | source)
XLA Modules:
  0.0 175.3 jit_solution(17535309687707718274)
XLA Ops:
  0.0 0.0 copy-start
  0.0 0.7 copy-done
  0.7 0.7 copy.13.head_gain
  1.4 171.9 %fused.1 = bf16[160,2048]{1,0:T(8,128)(2,1)} custom-call(bf16[160,2048]{1,0:T(8,128)(2,1)} %bitcast.9, bf16[1,128]{1,0:T(2,128)(2,1)} %cond.1, bf16[1,128]{1,0:T(2,128)(2,1)} %bitcast.13, bf16[32,2048]{1,0:T(8,128)(2,1)} %bitcast.10, bf16[3,128,512]{2,1,0:T(8,128)(2,1)} %w_mod.1, f32[1,2048]{1,0:T(1,128)} %bitcast.11, bf16[2048,2,128]{2,1,0:T(2,128)(2,1)} %w_query.1, ...), custom_call_target="tpu_custom_call" | custom-call | tf_op jit(solution)/shard_map/fused/pallas_call | solution.py:454
  173.3 2.0 %copy.15 = bf16[1,160,2048]{2,1,0:T(8,128)(2,1)} copy(bf16[1,160,2048]{2,1,0:T(8,128)(2,1)} %bitcast.7) | data formatting | bytes 1310720
Async XLA Ops:
  0.0 0.7 copy-start
